TPU v7x, 32 devices: a whole 2x2x4 slice. The times are simulated.
32 devices in a mesh: grp: 2 (over y), sp: 4 (over z), tp: 4 (over x, core).
Axes of the slice: x: 2, y: 2, z: 4, core: 2. Of those that a mesh axis runs over, the one named last changes fastest.
Arguments:
- residual: bfloat16 [2048, 2048], P(('grp', 'sp')), parts along dimension 0, may hold values from -34 to 34
- queries: bfloat16 [2048, 1024], P(('grp', 'sp'), 'tp'), parts along dimension 0, may hold values from -400 to 400
- keys: bfloat16 [2048, 512], P(('grp', 'sp'), 'tp'), parts along dimension 0, may hold values from -8 to 8
- values: bfloat16 [2048, 512], P(('grp', 'sp'), 'tp'), parts along dimension 0, may hold values from -6 to 6
- segments: int32 [2048], P(('grp', 'sp')), parts along dimension 0, may hold values from 0 to 2, never falling along the last dimension, each value on 1 to 768 neighbouring positions
- routes: int32 [2048, 2], P(('grp', 'sp')), parts along dimension 0, may hold values from 0 to 3, all different within a row; in each aligned block of 256 rows (0 to 255, 256 to 511, ...) at most 256 rows name the same one
- route_weight: float32 [2048, 2], P(('grp', 'sp')), parts along dimension 0, may hold values from 0.3 to 3
- sinks: float32 [16], P('tp'), may hold values from 1 to 6
- out_weight: bfloat16 [1024, 2048], P('tp'), may hold values from -1 to 1
- norm_gain: float32 [2048], replicated, may hold values from 0.1 to 1.9
- expert_gate: bfloat16 [4, 2048, 1024], P('sp', None, 'tp'), may hold values from -0.125 to 0.125
- expert_up: bfloat16 [4, 2048, 1024], P('sp', None, 'tp'), may hold values from -0.125 to 0.125
- expert_down: bfloat16 [4, 1024, 2048], P('sp', None, 'tp'), may hold values from -0.1875 to 0.1875
- shared_gate: bfloat16 [2048, 1024], P(None, 'tp'), may hold values from -0.125 to 0.125
- shared_up: bfloat16 [2048, 1024], P(None, 'tp'), may hold values from -0.125 to 0.125
- shared_down: bfloat16 [1024, 2048], P(None, 'tp'), may hold values from -0.1875 to 0.1875
Outputs:
- mixed: bfloat16 [2048, 2048], P(('grp', 'sp'), 'tp'), parts along dimension 0
There are 2 independent parts, one for each index of `grp`. A program takes and returns all parts, laid end to end along the dimension named above; an argument that names none is the same for every part. Nothing has to cross between parts.
Inputs may be any that keep to these rules, and one draw needn't show every extreme that they name: `routes`: each row names 2 different experts. In the rows of one device no expert is named by more than 256 rows, and in some device's rows an expert is named by exactly 256. `segments`: document numbers never fall along the positions; every document spans 1 to 768 positions and one spans exactly 768.
All inputs are finite; a program needn't handle non-finite values.
Results may differ from a plain program's by a relative error of at most 0.0065.
Values may be sent and summed in bfloat16 or wider, within the bound.
A program may use at most 64 MiB of HBM per device.

v0:
```python
import jax
import jax.numpy as jnp
from jax import lax
from jax.sharding import PartitionSpec as P

HEAD_DIM = 64
WINDOW = 128
epsilon = 1e-06


def passed_along(value, axis, steps):
    count = lax.axis_size(axis)
    leading, last = (max(0, -steps), min(count, count - steps))
    return lax.ppermute(value, axis, [(source, source + steps) for source in range(leading, last)])


def banded(prev_rows, own_rows, window_len):
    blocks = own_rows.shape[0] // window_len
    joined = jnp.concatenate([prev_rows, own_rows], axis=0)
    shaped = joined.reshape((blocks + 1, window_len) + own_rows.shape[1:])
    return jnp.concatenate([shaped[:-1], shaped[1:]], axis=1)


def shards(
    residual,
    queries,
    keys,
    values,
    segments,
    routes,
    route_weight,
    sinks,
    out_weight,
    norm_gain,
    expert_gate,
    expert_up,
    expert_down,
    shared_gate,
    shared_up,
    shared_down,
):
    rows_here = residual.shape[0]
    model_width = residual.shape[1]
    tp_count = lax.axis_size("tp")
    tp_index = lax.axis_index("tp")
    head_local = queries.shape[1] // HEAD_DIM
    kv_local = keys.shape[1] // HEAD_DIM
    group_size = head_local // kv_local
    window_len = WINDOW
    blocks = rows_here // window_len
    own_marks = (segments % 256 + 1).astype(jnp.bfloat16)
    prev_keys, prev_values, prev_marks = passed_along(
        (
            keys[rows_here - window_len :],
            values[rows_here - window_len :],
            own_marks[rows_here - window_len :],
        ),
        "sp",
        1,
    )
    key_band = banded(prev_keys, keys, window_len).reshape(
        blocks, 2 * window_len, kv_local, HEAD_DIM
    )
    value_band = banded(prev_values, values, window_len).reshape(
        blocks, 2 * window_len, kv_local, HEAD_DIM
    )
    mark_band = banded(prev_marks, own_marks, window_len).astype(jnp.float32)
    query_marks = own_marks.reshape(blocks, window_len).astype(jnp.float32)
    query_blocks = queries.reshape(blocks, window_len, kv_local, group_size, HEAD_DIM)
    scores = jnp.einsum(
        "nqhgd,nkhd->nhgqk", query_blocks, key_band, preferred_element_type=jnp.float32
    ) * HEAD_DIM ** (-0.5)
    offsets = jnp.arange(window_len)[:, None] + window_len - jnp.arange(2 * window_len)[None, :]
    allowed = (
        (offsets >= 0) & (offsets < window_len) & (query_marks[:, :, None] == mark_band[:, None, :])
    )
    sink_logits = sinks.reshape(kv_local, group_size)[None, :, :, None]
    masked = jnp.where(allowed[:, None, None], scores, -jnp.inf)
    top_score = jnp.maximum(jnp.max(masked, axis=-1), sink_logits)
    exp_terms = jnp.where(allowed[:, None, None], jnp.exp(scores - top_score[..., None]), 0.0)
    denominator = jnp.sum(exp_terms, axis=-1) + jnp.exp(sink_logits - top_score)
    probabilities = (exp_terms / denominator[..., None]).astype(jnp.bfloat16)
    attended = jnp.einsum(
        "nhgqk,nkhd->nqhgd", probabilities, value_band, preferred_element_type=jnp.float32
    )
    attended = attended.astype(jnp.bfloat16).reshape(rows_here, head_local * HEAD_DIM)
    partial_value = jnp.dot(attended, out_weight, preferred_element_type=jnp.float32)
    col_width = model_width // tp_count
    col_start = tp_index * col_width
    summed = lax.psum(partial_value, "tp")
    updated = (residual.astype(jnp.float32) + summed).astype(jnp.bfloat16)
    updated_f32 = updated.astype(jnp.float32)
    inv_rms = lax.rsqrt(jnp.mean(updated_f32 * updated_f32, axis=-1, keepdims=True) + epsilon)
    normed = (updated_f32 * inv_rms * norm_gain).astype(jnp.bfloat16)
    updated_cols = lax.dynamic_slice_in_dim(updated, col_start, col_width, 1)
    normed_cols = lax.dynamic_slice_in_dim(normed, col_start, col_width, 1)
    shared_pre = jnp.dot(normed, shared_gate, preferred_element_type=jnp.float32)
    shared_lin = jnp.dot(normed, shared_up, preferred_element_type=jnp.float32)
    shared_act = (jax.nn.silu(shared_pre) * shared_lin).astype(jnp.bfloat16)
    top_count = routes.shape[1]
    experts = lax.axis_size("sp")
    capacity = 2 * rows_here * top_count // experts
    flat_ids = routes.reshape(-1)
    one_hot = (flat_ids[:, None] == jnp.arange(experts, dtype=jnp.int32)[None, :]).astype(jnp.int32)
    rank_in = jnp.cumsum(one_hot, axis=0) - one_hot
    slot_dest = flat_ids * capacity + jnp.sum(rank_in * one_hot, axis=1)
    token_of = jnp.arange(rows_here * top_count, dtype=jnp.int32) // top_count
    slot_token = jnp.full((experts * capacity,), -1, jnp.int32).at[slot_dest].set(token_of)
    filled = slot_token >= 0
    safe_token = jnp.where(filled, slot_token, 0)
    outgoing = jnp.where(filled[:, None], normed_cols[safe_token], jnp.zeros((), jnp.bfloat16))
    pieces = lax.all_to_all(
        outgoing.reshape(experts, capacity, col_width),
        "sp",
        split_axis=0,
        concat_axis=0,
        tiled=True,
    )
    arrived = lax.all_gather(pieces, "tp", axis=2, tiled=True)
    expert_rows = arrived.reshape(-1, model_width)
    gate_pre = jnp.dot(expert_rows, expert_gate[0], preferred_element_type=jnp.float32)
    up_lin = jnp.dot(expert_rows, expert_up[0], preferred_element_type=jnp.float32)
    expert_act = (jax.nn.silu(gate_pre) * up_lin).astype(jnp.bfloat16)
    gathered_expert, gathered_shared = (
        lax.all_gather(expert_act, "tp", axis=1, tiled=True),
        lax.all_gather(shared_act, "tp", axis=1, tiled=True),
    )
    expert_out = jnp.dot(
        gathered_expert, expert_down[0], preferred_element_type=jnp.float32
    ).astype(jnp.bfloat16)
    returned = lax.all_to_all(
        expert_out.reshape(experts, capacity, col_width),
        "sp",
        split_axis=0,
        concat_axis=0,
        tiled=True,
    )
    returned = returned.reshape(experts * capacity, col_width)
    picked = returned[slot_dest].astype(jnp.float32).reshape(rows_here, top_count, col_width)
    routed = jnp.sum(picked * route_weight[:, :, None], axis=1)
    shared_cols = jnp.dot(gathered_shared, shared_down, preferred_element_type=jnp.float32)
    return (updated_cols.astype(jnp.float32) + shared_cols + routed).astype(jnp.bfloat16)


def solution(mesh):
    placed = (
        P(("grp", "sp"), None),
        P(("grp", "sp"), "tp"),
        P(("grp", "sp"), "tp"),
        P(("grp", "sp"), "tp"),
        P(("grp", "sp")),
        P(("grp", "sp"), None),
        P(("grp", "sp"), None),
        P("tp"),
        P("tp", None),
        P(),
        P("sp", None, "tp"),
        P("sp", None, "tp"),
        P("sp", None, "tp"),
        P(None, "tp"),
        P(None, "tp"),
        P(None, "tp"),
    )
    return jax.shard_map(
        shards, mesh=mesh, in_specs=placed, out_specs=P(("grp", "sp"), "tp"), check_vma=False
    )
```

profile of v0, /device:TPU:0, one launch (start us, length us, event | category | flops | bytes accessed | tf_op | source)
XLA Modules:
  0.0 231.0 jit_solution(2736606239957524361)
XLA Ops:
  6.5 0.8 bitcast_convert_fusion
  7.3 5.0 %collective-permute-start.1 = (bf16[128]{0:T(256)(128)(2,1)S(1)}, bf16[128]{0:T(256)(128)(2,1)S(1)}, u32[]{:S(2)}, u32[]{:S(2)}) collective-permute-start(bf16[128]{0:T(256)(128)(2,1)S(1)} %slice.47), channel_id=1, source_target_pairs={{0,4},{4,8},{8,12},{1,5},{5,9},{9,13},{2,6},{6,10},{10,14},{3,7},{... | collective-permute-start | bytes 776 | tf_op jit(solution)/shard_map/ppermute | solution.py:14
  12.3 0.8 slice.50
  13.1 3.5 %collective-permute-start.2 = (bf16[128,128]{1,0:T(8,128)(2,1)S(1)}, bf16[128,128]{1,0:T(8,128)(2,1)S(1)}, u32[]{:S(2)}, u32[]{:S(2)}) collective-permute-start(bf16[128,128]{1,0:T(8,128)(2,1)S(1)} %slice.50), channel_id=1, source_target_pairs={{0,4},{4,8},{8,12},{1,5},{5,9},{9,13},{2,6},{6,10},{10,14},{3,7},{... | collective-permute-start | bytes 98312 | tf_op jit(solution)/shard_map/ppermute | solution.py:14
  16.5 0.8 slice.45
  17.3 3.5 %collective-permute-start = (bf16[128,128]{1,0:T(8,128)(2,1)S(1)}, bf16[128,128]{1,0:T(8,128)(2,1)S(1)}, u32[]{:S(2)}, u32[]{:S(2)}) collective-permute-start(bf16[128,128]{1,0:T(8,128)(2,1)S(1)} %slice.45), channel_id=1, source_target_pairs={{0,4},{4,8},{8,12},{1,5},{5,9},{9,13},{2,6},{6,10},{10,14},{3,7},{... | collective-permute-start | bytes 98312 | tf_op jit(solution)/shard_map/ppermute | solution.py:14
  20.8 0.9 reshape.215
  21.7 0.9 reshape.213
  22.7 0.8 copy.33
  23.5 0.7 broadcast_multiply_fusion
  24.2 0.1 eq.51
  24.4 1.2 reduce-window.6
  25.6 0.2 slice_reduce_fusion
  25.8 1.1 reshape.216
  27.1 0.7 max.17
  28.0 0.1 compare_and_fusion
  28.1 0.8 pad_maximum_fusion
  29.1 0.4 select_reduce_fusion
  29.5 0.2 fusion.13
  30.1 0.4 fusion.8
  30.4 0.1 copy.31
  30.6 1.8 fusion.15
  32.5 0.1 eq.47
  32.6 0.2 reduce-window.9
  32.9 0.1 mul.85
  33.2 2.4 %scatter_custom_fusion = s32[1024]{0:T(1024)S(1)} fusion(s32[512]{0:T(512)S(1)} %bitcast.75, s32[512]{0:T(512)S(1)} %add_select_fusion, s32[]{:T(128)} %constant.70.clone.1), kind=kCustom, calls=%fused_computation.71 | custom fusion | bytes 4100 | tf_op jit(solution)/shard_map/scatter | solution.py:108
  35.7 46.5 %all-reduce.2.cloned.1.call-done = f32[256,2048]{1,0:T(8,128)} async-done(((f32[256,2048]{1,0:T(8,128)}), f32[256,2048]{1,0:T(8,128)}) %all-reduce.2.cloned.1.call-update) | async-done | bytes 2097168 | tf_op jit(solution)/shard_map/psum | solution.py:90
  82.2 2.0 fusion
  84.2 0.3 fusion.2
  84.5 1.0 copy-done.1
  85.5 4.0 %gather_fusion = bf16[1024,512]{1,0:T(8,128)(2,1)S(1)} fusion(bf16[256,512]{1,0:T(8,128)(2,1)S(1)} %constant_dynamic-slice_fusion, s32[1024]{0:T(1024)S(1)} %fusion.29), kind=kCustom, calls=%fused_computation | custom fusion | bytes 2101248 | tf_op jit(solution)/shard_map/gather | solution.py:111
  89.4 0.2 broadcast_select_fusion
  89.7 30.1 %all_to_all.10 = bf16[4,256,512]{2,1,0:T(8,128)(2,1)} all-to-all(bf16[4,256,512]{2,1,0:T(8,128)(2,1)S(1)} %broadcast_select_fusion), channel_id=1, replica_groups=mesh['grp'=2,'sp'=4,'tp'=4] {'sp'}, dimensions={0} | all-to-all | bytes 2097152 | tf_op jit(solution)/shard_map/all_to_all | solution.py:112
  119.9 32.9 %all-gather.3.cloned.1.call-done = bf16[4,256,2048]{2,1,0:T(8,128)(2,1)} async-done(((bf16[4,256,512]{2,1,0:T(8,128)(2,1)}), bf16[4,256,2048]{2,1,0:T(8,128)(2,1)}) %all-gather.3.cloned.1.call-update) | async-done | bytes 4194320 | tf_op jit(solution)/shard_map/all_gather | solution.py:119
  152.8 3.6 %fusion.11 = f32[1024,256]{1,0:T(8,128)S(1)} fusion(bf16[1024,2048]{1,0:T(8,128)(2,1)} %bitcast.80, bf16[1,2048,256]{2,1,0:T(8,128)(2,1)S(1)} %copy-done.8), kind=kOutput, calls=%fused_computation.23 | convolution fusion | flops 1073741824 | bytes 6291456 | tf_op jit(solution)/shard_map/dot_general | solution.py:121
  156.4 0.1 copy-done.9
  156.5 2.1 fusion.4
  158.6 23.0 %all-gather.5.cloned.1.call-done = bf16[1024,1024]{1,0:T(8,128)(2,1)} async-done(((bf16[1024,256]{1,0:T(8,128)(2,1)}), bf16[1024,1024]{1,0:T(8,128)(2,1)}) %all-gather.5.cloned.1.call-update) | async-done | bytes 2097168 | tf_op jit(solution)/shard_map/all_gather | solution.py:125
  181.6 3.9 %convolution_convert_fusion = bf16[1024,512]{1,0:T(8,128)(2,1)} fusion(bf16[1024,1024]{1,0:T(8,128)(2,1)} %all-gather.5.cloned.1.call-done, bf16[1,1024,512]{2,1,0:T(8,128)(2,1)S(1)} %copy-done.10), kind=kOutput, calls=%fused_computation.9 | convolution fusion | flops 1074266112 | bytes 4194304 | tf_op jit(solution)/shard_map/dot_general | solution.py:128
  185.5 4.7 %all-to-all-start.1 = ((bf16[4,256,512]{2,1,0:T(8,128)(2,1)}), bf16[4,256,512]{2,1,0:T(8,128)(2,1)S(1)}, u32[]{:S(2)}, u32[]{:S(2)}) async-start(bf16[4,256,512]{2,1,0:T(8,128)(2,1)} %bitcast.73), calls=%async_computation.1 | async-start | bytes 2097152 | tf_op jit(solution)/shard_map/all_to_all | solution.py:131
  190.3 2.1 fusion.42
  192.5 0.4 fusion.7
  192.9 7.5 %all_gather.9 = bf16[256,1024]{1,0:T(8,128)(2,1)} all-gather(bf16[256,256]{1,0:T(8,128)(2,1)S(1)} %fusion.7), channel_id=1, replica_groups=mesh['grp'=2,'sp'=4,'tp'=4] {'tp'}, dimensions={1}, use_global_device_ids=true | all-gather | bytes 655360 | tf_op jit(solution)/shard_map/all_gather | solution.py:126
  200.5 15.8 %all-to-all-done.1 = bf16[4,256,512]{2,1,0:T(8,128)(2,1)S(1)} async-done(((bf16[4,256,512]{2,1,0:T(8,128)(2,1)}), bf16[4,256,512]{2,1,0:T(8,128)(2,1)S(1)}, u32[]{:S(2)}, u32[]{:S(2)}) %all-to-all-start.1) | async-done | bytes 1048608 | tf_op jit(solution)/shard_map/all_to_all | solution.py:131
  216.3 2.6 %gather_fusion.1 = bf16[512,512]{1,0:T(8,128)(2,1)} fusion(bf16[1024,512]{1,0:T(8,128)(2,1)S(1)} %bitcast.71, s32[1024]{0:T(1024)S(1)} %pad_clamp_fusion), kind=kCustom, calls=%fused_computation.1 | custom fusion | bytes 1050624 | tf_op jit(solution)/shard_map/gather | solution.py:139
  218.9 1.7 reshape.184
  220.6 1.3 multiply_reduce_fusion
  222.0 2.5 %fusion.6 = bf16[256,512]{1,0:T(8,128)(2,1)} fusion(f32[256,512]{1,0:T(8,128)S(1)} %multiply_reduce_fusion, bf16[256,1024]{1,0:T(8,128)(2,1)} %all_gather.9, bf16[1024,512]{1,0:T(8,128)(2,1)} %param.31, bf16[256,2048]{1,0:T(8,128)(2,1)S(1)} %get-tuple-element.6, s32[]{:T(128)S(6)} %select_n.49), kind=kOutput, calls=%fused_computation.16 | convolution fusion | flops 268959744 | bytes 2621444 | tf_op jit(solution)/shard_map/dot_general | solution.py:141
  (59 shorter events, 1.5 us)
Async XLA Ops:
  6.5 24.1 %copy-start = (bf16[256,2048]{1,0:T(8,128)(2,1)S(1)}, bf16[256,2048]{1,0:T(8,128)(2,1)}, u32[]{:S(2)}) copy-start(bf16[256,2048]{1,0:T(8,128)(2,1)} %param.24) | copy-start | bytes 3145732
  6.5 75.6 %all-reduce.2.cloned.1.call-start = ((), (), s32[]{:S(2)}) async-start(), calls=%async_computation.2 | async-start | bytes 4194304 | tf_op jit(solution)/shard_map/psum | solution.py:90
  7.3 20.6 %collective-permute-start.1 = (bf16[128]{0:T(256)(128)(2,1)S(1)}, bf16[128]{0:T(256)(128)(2,1)S(1)}, u32[]{:S(2)}, u32[]{:S(2)}) collective-permute-start(bf16[128]{0:T(256)(128)(2,1)S(1)} %slice.47), channel_id=1, source_target_pairs={{0,4},{4,8},{8,12},{1,5},{5,9},{9,13},{2,6},{6,10},{10,14},{3,7},{... | collective-permute-start | bytes 776 | tf_op jit(solution)/shard_map/ppermute | solution.py:14
  13.1 15.0 %collective-permute-start.2 = (bf16[128,128]{1,0:T(8,128)(2,1)S(1)}, bf16[128,128]{1,0:T(8,128)(2,1)S(1)}, u32[]{:S(2)}, u32[]{:S(2)}) collective-permute-start(bf16[128,128]{1,0:T(8,128)(2,1)S(1)} %slice.50), channel_id=1, source_target_pairs={{0,4},{4,8},{8,12},{1,5},{5,9},{9,13},{2,6},{6,10},{10,14},{3,7},{... | collective-permute-start | bytes 98312 | tf_op jit(solution)/shard_map/ppermute | solution.py:14
  17.3 12.5 %collective-permute-start = (bf16[128,128]{1,0:T(8,128)(2,1)S(1)}, bf16[128,128]{1,0:T(8,128)(2,1)S(1)}, u32[]{:S(2)}, u32[]{:S(2)}) collective-permute-start(bf16[128,128]{1,0:T(8,128)(2,1)S(1)} %slice.45), channel_id=1, source_target_pairs={{0,4},{4,8},{8,12},{1,5},{5,9},{9,13},{2,6},{6,10},{10,14},{3,7},{... | collective-permute-start | bytes 98312 | tf_op jit(solution)/shard_map/ppermute | solution.py:14
  25.8 4.0 %copy-start.4 = (bf16[256,128]{1,0:T(8,128)(2,1)S(1)}, bf16[256,128]{1,0:T(8,128)(2,1)}, u32[]{:S(2)}) copy-start(bf16[256,128]{1,0:T(8,128)(2,1)} %param.19) | copy-start | bytes 196612
  32.4 49.8 %copy-start.3 = (bf16[256,2048]{1,0:T(8,128)(2,1)S(1)}, bf16[256,2048]{1,0:T(8,128)(2,1)}, u32[]{:S(2)}) copy-start(bf16[256,2048]{1,0:T(8,128)(2,1)} %param.16) | copy-start | bytes 3145732
  32.4 120.4 %all-gather.3.cloned.1.call-start = ((), (), s32[]{:S(2)}) async-start(), calls=%async_computation.3 | async-start | bytes 5242880 | tf_op jit(solution)/shard_map/all_gather | solution.py:119
  35.7 48.5 %copy-start.5 = (f32[2048]{0:T(1024)S(1)}, f32[2048]{0:T(1024)}, u32[]{:S(2)}) copy-start(f32[2048]{0:T(1024)} %param.25) | copy-start | bytes 24580
  84.5 1.0 copy-start.1
  89.6 63.1 %copy-start.8 = (bf16[1,2048,256]{2,1,0:T(8,128)(2,1)S(1)}, bf16[1,2048,256]{2,1,0:T(8,128)(2,1)}, u32[]{:S(2)}) copy-start(bf16[1,2048,256]{2,1,0:T(8,128)(2,1)} %param.26) | copy-start | bytes 3145732
  119.8 61.8 %all-gather.5.cloned.1.call-start = ((), (), s32[]{:S(2)}) async-start(), calls=%async_computation.4 | async-start | bytes 2621440 | tf_op jit(solution)/shard_map/all_gather | solution.py:125
  152.8 3.6 %copy-start.7 = (bf16[4,256,2048]{2,1,0:T(8,128)(2,1)S(1)}, bf16[4,256,2048]{2,1,0:T(8,128)(2,1)}, u32[]{:S(2)}) copy-start(bf16[4,256,2048]{2,1,0:T(8,128)(2,1)} %all-gather.3.cloned.1.call-done) | copy-start | bytes 12582916
  152.8 3.7 %copy-start.9 = (bf16[1,2048,256]{2,1,0:T(8,128)(2,1)S(1)}, bf16[1,2048,256]{2,1,0:T(8,128)(2,1)}, u32[]{:S(2)}) copy-start(bf16[1,2048,256]{2,1,0:T(8,128)(2,1)} %param.27) | copy-start | bytes 3145732
  156.5 25.1 %copy-start.10 = (bf16[1,1024,512]{2,1,0:T(8,128)(2,1)S(1)}, bf16[1,1024,512]{2,1,0:T(8,128)(2,1)}, u32[]{:S(2)}) copy-start(bf16[1,1024,512]{2,1,0:T(8,128)(2,1)} %param.28) | copy-start | bytes 3145732
  185.5 4.7 %copy-start.6 = (f32[256,2]{0,1:T(2,128)S(1)}, f32[256,2]{0,1:T(2,128)}, u32[]{:S(2)}) copy-start(f32[256,2]{0,1:T(2,128)} %param.22) | copy-start | bytes 6148
  185.5 30.8 %all-to-all-start.1 = ((bf16[4,256,512]{2,1,0:T(8,128)(2,1)}), bf16[4,256,512]{2,1,0:T(8,128)(2,1)S(1)}, u32[]{:S(2)}, u32[]{:S(2)}) async-start(bf16[4,256,512]{2,1,0:T(8,128)(2,1)} %bitcast.73), calls=%async_computation.1 | async-start | bytes 2097152 | tf_op jit(solution)/shard_map/all_to_all | solution.py:131
  190.3 2.2 copy-start.2
  190.3 2.2 copy-start.11
Sparse Core Ops, SparseCore 0:
  32.5 49.5 all-reduce.1
  119.9 32.7 all-gather.2
  158.8 22.8 all-gather.4
where the time goes:
time: 232 us; the launch traced here: 231 us
  waiting for transfers between devices  118 us (51%)
  blocking collectives  37.7 us (16%)
  local copies, waits for them, and re-layouts  19.6 us (8%)
  matrix products  17.1 us (7%)
  starting transfers between devices  16.7 us (7%)
  between operations  13.5 us (6%)
  other arithmetic  8.15 us (4%)
    psum x1, waiting for transfers between devices, shards(): summed = lax.psum(partial_value, 'tp')  46.5 us
    all_gather x1, waiting for transfers between devices, shards(): arrived = lax.all_gather(pieces, 'tp', axis=2, tiled=True)  32.9 us
    all_to_all x1, blocking collectives, shards(): lax.all_to_all(outgoing.reshape(experts, capacity, col_width), 'sp', spli...  30.1 us
    all_gather x1, waiting for transfers between devices, shards(): lax.all_gather(expert_act, 'tp', axis=1, tiled=True)  23 us
    all_to_all x1, waiting for transfers between devices, shards(): lax.all_to_all(expert_out.reshape(experts, capacity, col_width), 'sp', sp...  15.8 us
    ppermute x3, starting transfers between devices, passed_along(): lax.ppermute(value, axis, [(source, source + steps) for source in range(l...  11.9 us
    all_gather x1, blocking collectives, shards(): lax.all_gather(shared_act, 'tp', axis=1, tiled=True)  7.53 us
    all_to_all x1, starting transfers between devices, shards(): lax.all_to_all(expert_out.reshape(experts, capacity, col_width), 'sp', sp...  4.71 us
  transfers between devices with their start and end apart: 7, of which 4 were waited for; matrix products, arithmetic and copies ran while one was open for 7% of the time, Pallas kernels for 0%

commit v1 on v0

--- a/solution.py
+++ b/solution.py
@@ -87,7 +87,7 @@
     partial_value = jnp.dot(attended, out_weight, preferred_element_type=jnp.float32)
     col_width = model_width // tp_count
     col_start = tp_index * col_width
-    summed = lax.psum(partial_value, "tp")
+    summed = jnp.sum(lax.all_gather(partial_value, "tp"), axis=0)
     updated = (residual.astype(jnp.float32) + summed).astype(jnp.bfloat16)
     updated_f32 = updated.astype(jnp.float32)
     inv_rms = lax.rsqrt(jnp.mean(updated_f32 * updated_f32, axis=-1, keepdims=True) + epsilon)

time: 232 us -> 240 us (1.034)
  waiting for transfers between devices: 118 us -> 124 us
  other arithmetic: 8.15 us -> 11.5 us
    all_gather x0 -> x1, waiting for transfers between devices: none -> 51.6 us  [shards(): summed = jnp.sum(lax.all_gather(partial_value, 'tp'), axis=0)]
    psum x1 -> x0, waiting for transfers between devices: 46.5 us -> none  [shards(): summed = lax.psum(partial_value, 'tp')]
    reduce_sum x0 -> x1, other arithmetic: none -> 4.4 us  [shards(): summed = jnp.sum(lax.all_gather(partial_value, 'tp'), axis=0)]
  transfers between devices with their start and end apart: 7 -> 7, of which waited for: 4 -> 4; matrix products, arithmetic and copies ran while one was open for 7% -> 6% of each run, Pallas kernels for 0% -> 0%
where the time goes in v1:
time: 240 us; the launch traced here: 239 us
  waiting for transfers between devices  124 us (52%)
  blocking collectives  38.3 us (16%)
  local copies, waits for them, and re-layouts  19 us (8%)
  starting transfers between devices  16.7 us (7%)
  matrix products  16.7 us (7%)
  between operations  13.6 us (6%)
  other arithmetic  11.5 us (5%)
    all_gather x1, waiting for transfers between devices, shards(): summed = jnp.sum(lax.all_gather(partial_value, 'tp'), axis=0)  51.6 us
    all_gather x1, waiting for transfers between devices, shards(): arrived = lax.all_gather(pieces, 'tp', axis=2, tiled=True)  32.7 us
    all_to_all x1, blocking collectives, shards(): lax.all_to_all(outgoing.reshape(experts, capacity, col_width), 'sp', spli...  30.8 us
    all_gather x1, waiting for transfers between devices, shards(): lax.all_gather(expert_act, 'tp', axis=1, tiled=True)  23 us
    all_to_all x1, waiting for transfers between devices, shards(): lax.all_to_all(expert_out.reshape(experts, capacity, col_width), 'sp', sp...  16.2 us
    ppermute x3, starting transfers between devices, passed_along(): lax.ppermute(value, axis, [(source, source + steps) for source in range(l...  11.9 us
    all_gather x1, blocking collectives, shards(): lax.all_gather(shared_act, 'tp', axis=1, tiled=True)  7.54 us
  transfers between devices with their start and end apart: 7, of which 4 were waited for; matrix products, arithmetic and copies ran while one was open for 6% of the time, Pallas kernels for 0%

profile of v1, /device:TPU:0, one launch (start us, length us, event | category | flops | bytes accessed | tf_op | source)
XLA Modules:
  0.0 239.3 jit_solution(10419939031764097993)
XLA Ops:
  6.5 0.8 bitcast_convert_fusion
  7.3 5.0 %collective-permute-start.1 = (bf16[128]{0:T(256)(128)(2,1)S(1)}, bf16[128]{0:T(256)(128)(2,1)S(1)}, u32[]{:S(2)}, u32[]{:S(2)}) collective-permute-start(bf16[128]{0:T(256)(128)(2,1)S(1)} %slice.47), channel_id=1, source_target_pairs={{0,4},{4,8},{8,12},{1,5},{5,9},{9,13},{2,6},{6,10},{10,14},{3,7},{... | collective-permute-start | bytes 776 | tf_op jit(solution)/shard_map/ppermute | solution.py:14
  12.3 0.8 slice.50
  13.1 3.5 %collective-permute-start.2 = (bf16[128,128]{1,0:T(8,128)(2,1)S(1)}, bf16[128,128]{1,0:T(8,128)(2,1)S(1)}, u32[]{:S(2)}, u32[]{:S(2)}) collective-permute-start(bf16[128,128]{1,0:T(8,128)(2,1)S(1)} %slice.50), channel_id=1, source_target_pairs={{0,4},{4,8},{8,12},{1,5},{5,9},{9,13},{2,6},{6,10},{10,14},{3,7},{... | collective-permute-start | bytes 98312 | tf_op jit(solution)/shard_map/ppermute | solution.py:14
  16.5 0.8 slice.45
  17.3 3.5 %collective-permute-start = (bf16[128,128]{1,0:T(8,128)(2,1)S(1)}, bf16[128,128]{1,0:T(8,128)(2,1)S(1)}, u32[]{:S(2)}, u32[]{:S(2)}) collective-permute-start(bf16[128,128]{1,0:T(8,128)(2,1)S(1)} %slice.45), channel_id=1, source_target_pairs={{0,4},{4,8},{8,12},{1,5},{5,9},{9,13},{2,6},{6,10},{10,14},{3,7},{... | collective-permute-start | bytes 98312 | tf_op jit(solution)/shard_map/ppermute | solution.py:14
  20.8 0.9 reshape.216
  21.7 0.9 reshape.214
  22.7 1.1 reshape.217
  24.0 0.7 max.17
  24.9 0.1 compare_and_fusion
  25.0 0.8 pad_maximum_fusion
  26.0 0.4 select_reduce_fusion
  26.4 0.2 fusion.13
  27.0 0.4 fusion.8
  27.3 0.1 copy.31
  27.5 1.9 fusion.15
  29.6 0.1 eq.51
  29.7 0.1 eq.47
  29.9 1.2 reduce-window.6
  31.1 0.2 slice_reduce_fusion
  31.3 0.2 reduce-window.9
  31.5 0.1 copy.32
  31.7 0.1 mul.85
  31.9 2.4 %scatter_custom_fusion = s32[1024]{0:T(1024)S(1)} fusion(s32[512]{0:T(512)S(1)} %bitcast.77, s32[512]{0:T(512)S(1)} %add_select_fusion, s32[]{:T(128)} %constant.70.clone.1), kind=kCustom, calls=%fused_computation.71 | custom fusion | bytes 4100 | tf_op jit(solution)/shard_map/scatter | solution.py:108
  34.4 51.6 %all-gather.9.cloned.1.call-done = f32[1024,2048]{1,0:T(8,128)} async-done(((f32[256,2048]{1,0:T(8,128)}), f32[1024,2048]{1,0:T(8,128)}) %all-gather.9.cloned.1.call-update) | async-done | bytes 8388624 | tf_op jit(solution)/shard_map/all_gather | solution.py:90
  86.0 4.4 %reduce_sum.48 = f32[256,2048]{1,0:T(8,128)S(1)} reduce(f32[4,256,2048]{2,1,0:T(8,128)} %bitcast.73, f32[]{:T(128)} %constant.63.clone.1), dimensions={0}, to_apply=%region_2.3 | reduce | flops 1572864 | bytes 10485764 | tf_op jit(solution)/shard_map/reduce_sum | solution.py:90
  90.4 1.6 fusion
  92.1 1.0 copy-done.1
  93.0 0.3 fusion.2
  93.4 4.0 %gather_fusion = bf16[1024,512]{1,0:T(8,128)(2,1)S(1)} fusion(bf16[256,512]{1,0:T(8,128)(2,1)S(1)} %constant_dynamic-slice_fusion, s32[1024]{0:T(1024)S(1)} %fusion.29), kind=kCustom, calls=%fused_computation | custom fusion | bytes 2101248 | tf_op jit(solution)/shard_map/gather | solution.py:111
  97.3 0.2 broadcast_select_fusion
  97.6 30.8 %all_to_all.10 = bf16[4,256,512]{2,1,0:T(8,128)(2,1)} all-to-all(bf16[4,256,512]{2,1,0:T(8,128)(2,1)S(1)} %broadcast_select_fusion), channel_id=1, replica_groups=mesh['grp'=2,'sp'=4,'tp'=4] {'sp'}, dimensions={0} | all-to-all | bytes 2097152 | tf_op jit(solution)/shard_map/all_to_all | solution.py:112
  128.4 32.7 %all-gather.5.cloned.1.call-done = bf16[4,256,2048]{2,1,0:T(8,128)(2,1)} async-done(((bf16[4,256,512]{2,1,0:T(8,128)(2,1)}), bf16[4,256,2048]{2,1,0:T(8,128)(2,1)}) %all-gather.5.cloned.1.call-update) | async-done | bytes 4194320 | tf_op jit(solution)/shard_map/all_gather | solution.py:119
  161.1 3.6 %fusion.11 = f32[1024,256]{1,0:T(8,128)S(1)} fusion(bf16[1024,2048]{1,0:T(8,128)(2,1)} %bitcast.82, bf16[1,2048,256]{2,1,0:T(8,128)(2,1)S(1)} %copy-done.8), kind=kOutput, calls=%fused_computation.23 | convolution fusion | flops 1073741824 | bytes 6291456 | tf_op jit(solution)/shard_map/dot_general | solution.py:121
  164.7 0.1 copy-done.9
  164.9 2.1 fusion.4
  167.0 23.0 %all-gather.7.cloned.1.call-done = bf16[1024,1024]{1,0:T(8,128)(2,1)} async-done(((bf16[1024,256]{1,0:T(8,128)(2,1)}), bf16[1024,1024]{1,0:T(8,128)(2,1)}) %all-gather.7.cloned.1.call-update) | async-done | bytes 2097168 | tf_op jit(solution)/shard_map/all_gather | solution.py:125
  189.9 3.8 %convolution_convert_fusion = bf16[1024,512]{1,0:T(8,128)(2,1)} fusion(bf16[1024,1024]{1,0:T(8,128)(2,1)} %all-gather.7.cloned.1.call-done, bf16[1,1024,512]{2,1,0:T(8,128)(2,1)S(1)} %copy-done.10), kind=kOutput, calls=%fused_computation.9 | convolution fusion | flops 1074266112 | bytes 4194304 | tf_op jit(solution)/shard_map/dot_general | solution.py:128
  193.8 4.7 %all-to-all-start.1 = ((bf16[4,256,512]{2,1,0:T(8,128)(2,1)}), bf16[4,256,512]{2,1,0:T(8,128)(2,1)S(1)}, u32[]{:S(2)}, u32[]{:S(2)}) async-start(bf16[4,256,512]{2,1,0:T(8,128)(2,1)} %bitcast.75), calls=%async_computation.1 | async-start | bytes 2097152 | tf_op jit(solution)/shard_map/all_to_all | solution.py:131
  198.7 1.7 fusion.42
  200.4 0.4 fusion.7
  200.9 7.5 %all_gather.17 = bf16[256,1024]{1,0:T(8,128)(2,1)} all-gather(bf16[256,256]{1,0:T(8,128)(2,1)S(1)} %fusion.7), channel_id=1, replica_groups=mesh['grp'=2,'sp'=4,'tp'=4] {'tp'}, dimensions={1}, use_global_device_ids=true | all-gather | bytes 655360 | tf_op jit(solution)/shard_map/all_gather | solution.py:126
  208.4 16.2 %all-to-all-done.1 = bf16[4,256,512]{2,1,0:T(8,128)(2,1)S(1)} async-done(((bf16[4,256,512]{2,1,0:T(8,128)(2,1)}), bf16[4,256,512]{2,1,0:T(8,128)(2,1)S(1)}, u32[]{:S(2)}, u32[]{:S(2)}) %all-to-all-start.1) | async-done | bytes 1048608 | tf_op jit(solution)/shard_map/all_to_all | solution.py:131
  224.7 2.6 %gather_fusion.1 = bf16[512,512]{1,0:T(8,128)(2,1)} fusion(bf16[1024,512]{1,0:T(8,128)(2,1)S(1)} %bitcast.72, s32[1024]{0:T(1024)S(1)} %pad_clamp_fusion), kind=kCustom, calls=%fused_computation.1 | custom fusion | bytes 1050624 | tf_op jit(solution)/shard_map/gather | solution.py:139
  227.3 1.8 reshape.184
  229.0 1.3 multiply_reduce_fusion
  230.4 2.4 %fusion.6 = bf16[256,512]{1,0:T(8,128)(2,1)} fusion(f32[256,512]{1,0:T(8,128)S(1)} %multiply_reduce_fusion, bf16[256,1024]{1,0:T(8,128)(2,1)S(1)} %copy-done.2, bf16[1024,512]{1,0:T(8,128)(2,1)} %param.31, bf16[256,2048]{1,0:T(8,128)(2,1)} %copy-done.1, s32[]{:T(128)S(6)} %select_n.49), kind=kOutput, calls=%fused_computation.16 | convolution fusion | flops 268959744 | bytes 2621444 | tf_op jit(solution)/shard_map/dot_general | solution.py:141
  (60 shorter events, 1.5 us)
Async XLA Ops:
  6.5 21.0 %copy-start = (bf16[256,2048]{1,0:T(8,128)(2,1)S(1)}, bf16[256,2048]{1,0:T(8,128)(2,1)}, u32[]{:S(2)}) copy-start(bf16[256,2048]{1,0:T(8,128)(2,1)} %param.24) | copy-start | bytes 3145732
  6.5 79.5 %all-gather.9.cloned.1.call-start = ((), (), s32[]{:S(2)}) async-start(), calls=%async_computation.4 | async-start | bytes 10485760 | tf_op jit(solution)/shard_map/all_gather | solution.py:90
  7.3 17.5 %collective-permute-start.1 = (bf16[128]{0:T(256)(128)(2,1)S(1)}, bf16[128]{0:T(256)(128)(2,1)S(1)}, u32[]{:S(2)}, u32[]{:S(2)}) collective-permute-start(bf16[128]{0:T(256)(128)(2,1)S(1)} %slice.47), channel_id=1, source_target_pairs={{0,4},{4,8},{8,12},{1,5},{5,9},{9,13},{2,6},{6,10},{10,14},{3,7},{... | collective-permute-start | bytes 776 | tf_op jit(solution)/shard_map/ppermute | solution.py:14
  13.1 12.0 %collective-permute-start.2 = (bf16[128,128]{1,0:T(8,128)(2,1)S(1)}, bf16[128,128]{1,0:T(8,128)(2,1)S(1)}, u32[]{:S(2)}, u32[]{:S(2)}) collective-permute-start(bf16[128,128]{1,0:T(8,128)(2,1)S(1)} %slice.50), channel_id=1, source_target_pairs={{0,4},{4,8},{8,12},{1,5},{5,9},{9,13},{2,6},{6,10},{10,14},{3,7},{... | collective-permute-start | bytes 98312 | tf_op jit(solution)/shard_map/ppermute | solution.py:14
  17.3 9.4 %collective-permute-start = (bf16[128,128]{1,0:T(8,128)(2,1)S(1)}, bf16[128,128]{1,0:T(8,128)(2,1)S(1)}, u32[]{:S(2)}, u32[]{:S(2)}) collective-permute-start(bf16[128,128]{1,0:T(8,128)(2,1)S(1)} %slice.45), channel_id=1, source_target_pairs={{0,4},{4,8},{8,12},{1,5},{5,9},{9,13},{2,6},{6,10},{10,14},{3,7},{... | collective-permute-start | bytes 98312 | tf_op jit(solution)/shard_map/ppermute | solution.py:14
  22.7 4.0 %copy-start.3 = (bf16[256,128]{1,0:T(8,128)(2,1)S(1)}, bf16[256,128]{1,0:T(8,128)(2,1)}, u32[]{:S(2)}) copy-start(bf16[256,128]{1,0:T(8,128)(2,1)} %param.19) | copy-start | bytes 196612
  27.5 1.9 copy-start.5
  29.4 131.7 %all-gather.5.cloned.1.call-start = ((), (), s32[]{:S(2)}) async-start(), calls=%async_computation.2 | async-start | bytes 5242880 | tf_op jit(solution)/shard_map/all_gather | solution.py:119
  90.4 2.6 %copy-start.4 = (f32[2048]{0:T(1024)S(1)}, f32[2048]{0:T(1024)}, u32[]{:S(2)}) copy-start(f32[2048]{0:T(1024)} %param.25) | copy-start | bytes 24580
  92.1 1.0 copy-start.1
  97.6 63.6 %copy-start.8 = (bf16[1,2048,256]{2,1,0:T(8,128)(2,1)S(1)}, bf16[1,2048,256]{2,1,0:T(8,128)(2,1)}, u32[]{:S(2)}) copy-start(bf16[1,2048,256]{2,1,0:T(8,128)(2,1)} %param.26) | copy-start | bytes 3145732
  128.4 61.6 %all-gather.7.cloned.1.call-start = ((), (), s32[]{:S(2)}) async-start(), calls=%async_computation.3 | async-start | bytes 2621440 | tf_op jit(solution)/shard_map/all_gather | solution.py:125
  161.1 3.6 %copy-start.7 = (bf16[4,256,2048]{2,1,0:T(8,128)(2,1)S(1)}, bf16[4,256,2048]{2,1,0:T(8,128)(2,1)}, u32[]{:S(2)}) copy-start(bf16[4,256,2048]{2,1,0:T(8,128)(2,1)} %all-gather.5.cloned.1.call-done) | copy-start | bytes 12582916
  161.1 3.7 %copy-start.9 = (bf16[1,2048,256]{2,1,0:T(8,128)(2,1)S(1)}, bf16[1,2048,256]{2,1,0:T(8,128)(2,1)}, u32[]{:S(2)}) copy-start(bf16[1,2048,256]{2,1,0:T(8,128)(2,1)} %param.27) | copy-start | bytes 3145732
  164.9 25.1 %copy-start.10 = (bf16[1,1024,512]{2,1,0:T(8,128)(2,1)S(1)}, bf16[1,1024,512]{2,1,0:T(8,128)(2,1)}, u32[]{:S(2)}) copy-start(bf16[1,1024,512]{2,1,0:T(8,128)(2,1)} %param.28) | copy-start | bytes 3145732
  193.8 4.7 %copy-start.6 = (f32[256,2]{0,1:T(2,128)S(1)}, f32[256,2]{0,1:T(2,128)}, u32[]{:S(2)}) copy-start(f32[256,2]{0,1:T(2,128)} %param.22) | copy-start | bytes 6148
  193.8 30.9 %all-to-all-start.1 = ((bf16[4,256,512]{2,1,0:T(8,128)(2,1)}), bf16[4,256,512]{2,1,0:T(8,128)(2,1)S(1)}, u32[]{:S(2)}, u32[]{:S(2)}) async-start(bf16[4,256,512]{2,1,0:T(8,128)(2,1)} %bitcast.75), calls=%async_computation.1 | async-start | bytes 2097152 | tf_op jit(solution)/shard_map/all_to_all | solution.py:131
  198.6 1.8 copy-start.11
  227.3 3.1 %copy-start.2 = (bf16[256,1024]{1,0:T(8,128)(2,1)S(1)}, bf16[256,1024]{1,0:T(8,128)(2,1)}, u32[]{:S(2)}) copy-start(bf16[256,1024]{1,0:T(8,128)(2,1)} %all_gather.17) | copy-start | bytes 1572868
Sparse Core Ops, SparseCore 0:
  29.5 56.4 all-gather.8
  128.5 32.5 all-gather.4
  167.1 22.8 all-gather.6
